TPU v7x, 128 devices: a 2x2x16 block of a 8x8x16 slice. The times are simulated.
128 devices in a mesh: grp: 4 (over y, x), ep: 32 (over z, core).
Axes of the slice: x: 2, y: 2, z: 16, core: 2. Of those that a mesh axis runs over, the one named last changes fastest.
The devices are a block of a 8x8x16 slice.
Arguments:
- hidden: bfloat16 [1024, 2048], P(('grp', 'ep')), parts along dimension 0, may hold values from -6 to 6
- norm_gain: bfloat16 [2048], replicated, may hold values from 0.099609375 to 1.8984375
- outgate_weight: bfloat16 [2048, 2048], P(None, 'ep'), may hold values from -0.125 to 0.125
- input_weight: bfloat16 [2048, 2048], P(None, 'ep'), may hold values from -0.125 to 0.125
- write_weight: bfloat16 [2048, 512], P(None, 'ep'), may hold values from -0.125 to 0.125
- read_weight: bfloat16 [2048, 512], P(None, 'ep'), may hold values from -0.125 to 0.125
- step_weight: bfloat16 [2048, 32], replicated, may hold values from -0.125 to 0.125
- step_bias: float32 [32], replicated, may hold values from -1.5 to 1
- decay_log: float32 [32], replicated, may hold values from -3 to 1
- skip_gain: float32 [32], replicated, may hold values from 0.1 to 1.9
- conv_weight: bfloat16 [4, 3072], replicated, may hold values from -3 to 3
- conv_state: bfloat16 [1024, 3, 3072], P(('grp', 'ep')), parts along dimension 0, may hold values from -6 to 6
- mixer_state: float32 [1024, 32, 64, 128], P(('grp', 'ep')), parts along dimension 0, may hold values from -3 to 3
- inner_gain: bfloat16 [2048], replicated, may hold values from 0.099609375 to 1.8984375
- out_weight: bfloat16 [2048, 2048], P('ep'), may hold values from -0.125 to 0.125
- ffn_gain: bfloat16 [2048], replicated, may hold values from 0.099609375 to 1.8984375
- expert_gate: bfloat16 [2048, 28672], P(None, 'ep'), may hold values from -0.125 to 0.125
- expert_up: bfloat16 [2048, 28672], P(None, 'ep'), may hold values from -0.125 to 0.125
- expert_down: bfloat16 [28672, 2048], P('ep'), may hold values from -0.09375 to 0.09375
- route_ids: int32 [1024, 2], P(('grp', 'ep')), parts along dimension 0, may hold values from 0 to 7, all different within a row; in each aligned block of 8 rows (0 to 7, 8 to 15, ...) at most 8 rows name the same one
- route_weights: float32 [1024, 2], P(('grp', 'ep')), parts along dimension 0, may hold values from 0.1 to 1
Outputs:
- result: bfloat16 [1024, 2048], P(('grp', 'ep')), parts along dimension 0
- new_state: float32 [1024, 32, 64, 128], P(('grp', 'ep')), parts along dimension 0
- new_conv: bfloat16 [1024, 3, 3072], P(('grp', 'ep')), parts along dimension 0
There are 4 independent parts, one for each index of `grp`. A program takes and returns all parts, laid end to end along the dimension named above; an argument that names none is the same for every part. Nothing has to cross between parts.
Inputs may be any that keep to these rules, and one draw needn't show every extreme that they name: `route_ids`: each row names 2 different experts; the rows of one device name one expert at most 8 times.
All inputs are finite; a program needn't handle non-finite values.
Results may differ from a plain program's by a relative error of at most 0.02.
Values may be sent and summed in bfloat16 or wider, within the bound.
A program may use at most 128 MiB of HBM per device.

v0:
```python
import jax
import jax.numpy as jnp
from jax import lax
from jax.sharding import Mesh
from jax.sharding import PartitionSpec as P

EXPERTS = 8
EP = ("ep_0", "ep_1")
GRP_EP = ("grp", "ep_0", "ep_1")


norm_eps = 1e-06


def in_order(parts, dim):
    parts = jnp.moveaxis(parts, 0, dim)
    lengths = parts.shape
    return parts.reshape(*lengths[:dim], lengths[dim] * lengths[dim + 1], *lengths[dim + 2 :])


def all_blocks(shard, axes, order):
    parts = shard
    for k in order:
        parts = lax.all_gather(parts, axes[k])
    done = order[::-1]
    back = [done.index(k) for k in range(len(axes))]
    parts = parts.transpose(*back, *range(len(axes), parts.ndim))
    return parts.reshape(-1, *shard.shape)


def gathered_by_axis(shard, axes, order, dim):
    return in_order(all_blocks(shard, axes, order), dim)


def split_up(shard, dim, length):
    lengths = shard.shape
    parts = shard.reshape(*lengths[:dim], length, lengths[dim] // length, *lengths[dim + 1 :])
    return jnp.moveaxis(parts, dim, 0)


def sum_at_owner(shard, axis, dim):
    parts = split_up(shard, dim, lax.axis_size(axis))
    arrived = lax.all_to_all(parts, axis, split_axis=0, concat_axis=0, tiled=True)
    return arrived.astype(jnp.float32).sum(axis=0)


def rms_scale(values, gain_vec):
    floats = values.astype(jnp.float32)
    scaled = floats * lax.rsqrt(jnp.mean(floats * floats, axis=-1, keepdims=True) + norm_eps)
    return scaled * gain_vec.astype(jnp.float32)


def mixer_step(
    gate_proj,
    input_proj,
    write_proj,
    read_proj,
    step_raw,
    step_bias,
    decay_log,
    skip_gain,
    conv_weight,
    conv_state,
    mixer_state,
    inner_gain,
):
    seqs_here, head_count, head_dim, state_width = mixer_state.shape
    group_count = write_proj.shape[1] // state_width
    per_group = head_count // group_count
    inner_width = head_count * head_dim
    new_row = jnp.concatenate([input_proj, write_proj, read_proj], axis=1)
    window = jnp.concatenate([conv_state, new_row[:, None, :]], axis=1)
    conv_out = jax.nn.silu(
        jnp.sum(window.astype(jnp.float32) * conv_weight.astype(jnp.float32)[None], axis=1)
    )
    conv_inputs = conv_out[:, :inner_width].reshape(seqs_here, group_count, per_group, head_dim)
    split_at = inner_width + group_count * state_width
    write_map = conv_out[:, inner_width:split_at].reshape(seqs_here, group_count, state_width)
    read_map = conv_out[:, split_at:].reshape(seqs_here, group_count, state_width)
    step_size = jax.nn.softplus(step_raw + step_bias)
    decay_rate = jnp.exp(-step_size * jnp.exp(decay_log)).reshape(seqs_here, group_count, per_group)
    scaled_inputs = conv_inputs * step_size.reshape(seqs_here, group_count, per_group)[..., None]
    old_state = mixer_state.reshape(seqs_here, group_count, per_group, head_dim, state_width)
    new_state = decay_rate[..., None, None] * old_state + jnp.einsum(
        "sgrp,sgn->sgrpn", scaled_inputs, write_map
    )
    read_out = jnp.einsum("sgrpn,sgn->sgrp", new_state, read_map)
    read_out = read_out + skip_gain.reshape(group_count, per_group)[None, :, :, None] * conv_inputs
    gated_in = read_out.reshape(seqs_here, inner_width) * jax.nn.silu(gate_proj.astype(jnp.float32))
    gated = rms_scale(gated_in, inner_gain).astype(jnp.bfloat16)
    return (gated, new_state.reshape(mixer_state.shape), window[:, 1:])


def on_device(
    hidden,
    norm_gain,
    outgate_weight,
    input_weight,
    write_weight,
    read_weight,
    step_weight,
    step_bias,
    decay_log,
    skip_gain,
    conv_weight,
    conv_state,
    mixer_state,
    inner_gain,
    out_weight,
    ffn_gain,
    expert_gate,
    expert_up,
    expert_down,
    route_ids,
    route_weights,
):
    devices = lax.axis_size(EP)
    normed = rms_scale(hidden, norm_gain).astype(jnp.bfloat16)
    all_rows = gathered_by_axis(normed, EP, (0, 1), 0)
    gate_cols = jnp.dot(all_rows, outgate_weight, preferred_element_type=jnp.float32).astype(
        jnp.bfloat16
    )
    input_cols = jnp.dot(all_rows, input_weight, preferred_element_type=jnp.float32).astype(
        jnp.bfloat16
    )
    write_cols = jnp.dot(all_rows, write_weight, preferred_element_type=jnp.float32).astype(
        jnp.bfloat16
    )
    read_cols = jnp.dot(all_rows, read_weight, preferred_element_type=jnp.float32).astype(
        jnp.bfloat16
    )
    gate_proj, input_proj, write_proj, read_proj = (
        lax.all_to_all(gate_cols, EP, split_axis=0, concat_axis=1, tiled=True),
        lax.all_to_all(input_cols, EP, split_axis=0, concat_axis=1, tiled=True),
        lax.all_to_all(write_cols, EP, split_axis=0, concat_axis=1, tiled=True),
        lax.all_to_all(read_cols, EP, split_axis=0, concat_axis=1, tiled=True),
    )
    step_raw = jnp.dot(normed, step_weight, preferred_element_type=jnp.float32)
    gated, new_state, new_conv = mixer_step(
        gate_proj,
        input_proj,
        write_proj,
        read_proj,
        step_raw,
        step_bias,
        decay_log,
        skip_gain,
        conv_weight,
        conv_state,
        mixer_state,
        inner_gain,
    )
    head_part = lax.all_to_all(gated, EP, split_axis=1, concat_axis=0, tiled=True)
    mixed_out = sum_at_owner(
        jnp.dot(head_part, out_weight, preferred_element_type=jnp.float32).astype(jnp.bfloat16),
        EP,
        0,
    )
    residual = (hidden.astype(jnp.float32) + mixed_out).astype(jnp.bfloat16)
    normed_ffn = rms_scale(residual, ffn_gain).astype(jnp.bfloat16)
    expert_split = devices // EXPERTS
    dest_expert = jnp.arange(devices, dtype=jnp.int32) // expert_split
    matches = route_ids[None, :, :] == dest_expert[:, None, None]
    slot_weight = jnp.sum(
        jnp.where(matches, route_weights[None], jnp.zeros((), jnp.float32)), axis=2
    )
    routed = jnp.any(matches, axis=2)
    send_rows = jnp.where(routed[..., None], normed_ffn[None], jnp.zeros((), jnp.bfloat16))
    token_rows = lax.all_to_all(send_rows, EP, split_axis=0, concat_axis=0, tiled=True)
    gate_part = jnp.einsum(
        "abi,if->abf", token_rows, expert_gate, preferred_element_type=jnp.float32
    )
    up_part = jnp.einsum("abi,if->abf", token_rows, expert_up, preferred_element_type=jnp.float32)
    units = (jax.nn.silu(gate_part) * up_part).astype(jnp.bfloat16)
    expert_out = jnp.einsum("abf,fi->abi", units, expert_down, preferred_element_type=jnp.float32)
    returned = lax.all_to_all(
        expert_out.astype(jnp.bfloat16), EP, split_axis=0, concat_axis=0, tiled=True
    ).astype(expert_out.dtype)
    moe_sum = jnp.sum(returned * slot_weight[..., None], axis=0)
    result = (residual.astype(jnp.float32) + moe_sum).astype(jnp.bfloat16)
    return (result, new_state, new_conv)


def solution(mesh):
    torus = Mesh(mesh.devices.reshape(mesh.shape["grp"], 16, 2), ("grp", "ep_0", "ep_1"))
    return jax.shard_map(
        on_device,
        mesh=torus,
        in_specs=(
            P(GRP_EP, None),
            P(),
            P(None, EP),
            P(None, EP),
            P(None, EP),
            P(None, EP),
            P(),
            P(),
            P(),
            P(),
            P(),
            P(GRP_EP, None, None),
            P(GRP_EP, None, None, None),
            P(),
            P(EP, None),
            P(),
            P(None, EP),
            P(None, EP),
            P(EP, None),
            P(GRP_EP, None),
            P(GRP_EP, None),
        ),
        out_specs=(P(GRP_EP, None), P(GRP_EP, None, None, None), P(GRP_EP, None, None)),
        check_vma=False,
    )
```

profile of v0, /device:TPU:196, one launch (start us, length us, event | category | flops | bytes accessed | tf_op | source)
XLA Modules:
  0.0 367.6 jit_solution(3995007156528579524)
XLA Ops:
  7.3 0.8 convert_element_type.79
  8.1 0.9 fusion.29
  9.0 0.8 fusion.31
  9.8 41.3 %all-gather = bf16[128,2048]{1,0:T(8,128)(2,1)} all-gather(bf16[8,2048]{1,0:T(8,128)(2,1)S(1)} %fusion.31), channel_id=2, replica_groups=mesh['grp'=4,'ep_0'=16,'ep_1'=2] {'ep_0'}, dimensions={0}, use_global_device_ids=true | all-gather | bytes 557056 | tf_op jit(solution)/shard_map/all_gather | solution.py:24
  51.1 0.8 convert_element_type.85
  52.6 1.1 multiply_exponential_fusion
  53.8 0.8 mul.160
  54.6 0.8 reshape.116
  55.3 9.1 %all-gather.4.cloned.1.call-done = bf16[32,8,2048]{2,1,0:T(8,128)(2,1)} async-done(((bf16[16,8,2048]{2,1,0:T(8,128)(2,1)}), bf16[32,8,2048]{2,1,0:T(8,128)(2,1)}) %all-gather.4.cloned.1.call-update) | async-done | bytes 1048592 | tf_op jit(solution)/shard_map/all_gather | solution.py:24
  64.5 1.3 copy.68
  66.2 0.8 copy.71
  66.9 12.7 %all-to-all-start.1 = ((bf16[32,8,16]{2,1,0:T(8,128)(2,1)}), bf16[32,8,16]{2,1,0:T(8,128)(2,1)S(1)}, u32[]{:S(2)}, u32[]{:S(2)}) async-start(bf16[32,8,16]{2,1,0:T(8,128)(2,1)} %bitcast.7), calls=%async_computation.1 | async-start | bytes 131072 | tf_op jit(solution)/shard_map/all_to_all | solution.py:135
  80.0 0.8 copy.73
  80.7 11.5 %all-to-all-done.1 = bf16[32,8,16]{2,1,0:T(8,128)(2,1)S(1)} async-done(((bf16[32,8,16]{2,1,0:T(8,128)(2,1)}), bf16[32,8,16]{2,1,0:T(8,128)(2,1)S(1)}, u32[]{:S(2)}, u32[]{:S(2)}) %all-to-all-start.1) | async-done | bytes 8224 | tf_op jit(solution)/shard_map/all_to_all | solution.py:135
  92.3 5.5 %all-to-all-start.2 = ((bf16[32,8,16]{2,1,0:T(8,128)(2,1)}), bf16[32,8,16]{2,1,0:T(8,128)(2,1)S(1)}, u32[]{:S(2)}, u32[]{:S(2)}) async-start(bf16[32,8,16]{2,1,0:T(8,128)(2,1)} %bitcast.9), calls=%async_computation.2 | async-start | bytes 131072 | tf_op jit(solution)/shard_map/all_to_all | solution.py:136
  98.3 0.7 reshape.124
  99.1 11.9 %all-to-all-done.2 = bf16[32,8,16]{2,1,0:T(8,128)(2,1)S(1)} async-done(((bf16[32,8,16]{2,1,0:T(8,128)(2,1)}), bf16[32,8,16]{2,1,0:T(8,128)(2,1)S(1)}, u32[]{:S(2)}, u32[]{:S(2)}) %all-to-all-start.2) | async-done | bytes 8224 | tf_op jit(solution)/shard_map/all_to_all | solution.py:136
  110.9 5.2 %all-to-all-start = ((bf16[32,2,256]{2,1,0:T(2,128)(2,1)}), bf16[32,2,256]{2,1,0:T(2,128)(2,1)S(1)}, u32[]{:S(2)}, u32[]{:S(2)}) async-start(bf16[32,2,256]{2,1,0:T(2,128)(2,1)} %reshape.124), calls=%async_computation | async-start | bytes 65536 | tf_op jit(solution)/shard_map/all_to_all | solution.py:134
  117.7 10.2 %all-to-all-done = bf16[32,2,256]{2,1,0:T(2,128)(2,1)S(1)} async-done(((bf16[32,2,256]{2,1,0:T(2,128)(2,1)}), bf16[32,2,256]{2,1,0:T(2,128)(2,1)S(1)}, u32[]{:S(2)}, u32[]{:S(2)}) %all-to-all-start) | async-done | bytes 32800 | tf_op jit(solution)/shard_map/all_to_all | solution.py:134
  127.9 5.1 %all-to-all-start.3 = ((bf16[32,2,256]{2,1,0:T(2,128)(2,1)}), bf16[32,2,256]{2,1,0:T(2,128)(2,1)S(1)}, u32[]{:S(2)}, u32[]{:S(2)}) async-start(bf16[32,2,256]{2,1,0:T(2,128)(2,1)} %reshape.126), calls=%async_computation.3 | async-start | bytes 65536 | tf_op jit(solution)/shard_map/all_to_all | solution.py:133
  133.6 11.3 %all-to-all-done.3 = bf16[32,2,256]{2,1,0:T(2,128)(2,1)S(1)} async-done(((bf16[32,2,256]{2,1,0:T(2,128)(2,1)}), bf16[32,2,256]{2,1,0:T(2,128)(2,1)S(1)}, u32[]{:S(2)}, u32[]{:S(2)}) %all-to-all-start.3) | async-done | bytes 32800 | tf_op jit(solution)/shard_map/all_to_all | solution.py:133
  145.1 5.5 %multiply_add_fusion = f32[8,4,8,64,128]{4,3,2,1,0:T(8,128)S(1)} fusion(f32[8,4,8,64,128]{4,3,2,1,0:T(8,128)} %bitcast.99, f32[8,4,128]{2,1,0:T(4,128)S(1)} %copy.75, f32[8,4,8,64]{3,2,1,0:T(8,128)S(1)} %broadcast_multiply_fusion, f32[8,4,8]{2,1,0:T(4,128)S(1)} %mul.151), kind=kLoop, calls=%fused_computation | loop fusion | flops 6291456 | bytes 16860160 | tf_op jit(solution)/shard_map/add | solution.py:84
  150.6 3.3 fusion.39
  154.4 16.0 %all_to_all.101 = bf16[32,2,256]{2,1,0:T(2,128)(2,1)S(1)} all-to-all(bf16[32,2,256]{2,1,0:T(2,128)(2,1)S(1)} %reshape.128), channel_id=1, replica_groups=mesh['grp'=4,'ep_0'=16,'ep_1'=2] {'ep_0','ep_1'}, dimensions={0} | all-to-all | bytes 65536 | tf_op jit(solution)/shard_map/all_to_all | solution.py:153
  170.6 1.4 fusion.9
  172.0 5.2 %all-to-all-start.5 = ((bf16[32,8,2048]{2,1,0:T(8,128)(2,1)}), bf16[32,8,2048]{2,1,0:T(8,128)(2,1)S(1)}, u32[]{:S(2)}, u32[]{:S(2)}) async-start(bf16[32,8,2048]{2,1,0:T(8,128)(2,1)} %fusion.9), calls=%async_computation.5 | async-start | bytes 2097152 | tf_op jit(solution)/shard_map/all_to_all | solution.py:43
  177.4 53.6 %all-to-all-done.5 = bf16[32,8,2048]{2,1,0:T(8,128)(2,1)S(1)} async-done(((bf16[32,8,2048]{2,1,0:T(8,128)(2,1)}), bf16[32,8,2048]{2,1,0:T(8,128)(2,1)S(1)}, u32[]{:S(2)}, u32[]{:S(2)}) %all-to-all-start.5) | async-done | bytes 1048608 | tf_op jit(solution)/shard_map/all_to_all | solution.py:43
  231.5 59.9 %all_to_all.102 = bf16[32,8,2048]{2,1,0:T(8,128)(2,1)S(1)} all-to-all(bf16[32,8,2048]{2,1,0:T(8,128)(2,1)S(1)} %broadcast_select_fusion), channel_id=1, replica_groups=mesh['grp'=4,'ep_0'=16,'ep_1'=2] {'ep_0','ep_1'}, dimensions={0} | all-to-all | bytes 2097152 | tf_op jit(solution)/shard_map/all_to_all | solution.py:169
  291.5 1.3 fusion.4
  292.8 6.5 %fusion.6 = bf16[32,8,2048]{2,1,0:T(8,128)(2,1)} fusion(bf16[896,2048]{1,0:T(8,128)(2,1)} %param.39, bf16[32,8,2048]{2,1,0:T(8,128)(2,1)S(1)} %all_to_all.102, bf16[2048,896]{1,0:T(8,128)(2,1)} %param.38, f32[32,8,896]{2,1,0:T(8,128)S(1)} %fusion.4), kind=kOutput, calls=%fused_computation.7 | convolution fusion | flops 1880948736 | bytes 10354688 | tf_op jit(solution)/shard_map/abf,fi->abi/dot_general | solution.py:175
  299.3 6.8 %all-to-all-start.7 = ((bf16[32,8,2048]{2,1,0:T(8,128)(2,1)}), bf16[32,8,2048]{2,1,0:T(8,128)(2,1)S(1)}, u32[]{:S(2)}, u32[]{:S(2)}) async-start(bf16[32,8,2048]{2,1,0:T(8,128)(2,1)} %fusion.6), calls=%async_computation.7 | async-start | bytes 2097152 | tf_op jit(solution)/shard_map/all_to_all | solution.py:176
  306.9 53.0 %all-to-all-done.7 = bf16[32,8,2048]{2,1,0:T(8,128)(2,1)S(1)} async-done(((bf16[32,8,2048]{2,1,0:T(8,128)(2,1)}), bf16[32,8,2048]{2,1,0:T(8,128)(2,1)S(1)}, u32[]{:S(2)}, u32[]{:S(2)}) %all-to-all-start.7) | async-done | bytes 1048608 | tf_op jit(solution)/shard_map/all_to_all | solution.py:176
  (74 shorter events, 7.6 us)
Async XLA Ops:
  7.2 163.4 %copy-start = (bf16[64,2048]{1,0:T(8,128)(2,1)S(1)}, bf16[64,2048]{1,0:T(8,128)(2,1)}, u32[]{:S(2)}) copy-start(bf16[64,2048]{1,0:T(8,128)(2,1)} %param.35) | copy-start | bytes 786436
  7.2 58.6 %copy-start.6 = (bf16[2048,16]{0,1:T(8,128)(2,1)S(1)}, bf16[2048,16]{0,1:T(8,128)(2,1)}, u32[]{:S(2)}) copy-start(bf16[2048,16]{0,1:T(8,128)(2,1)} %param.25) | copy-start | bytes 196612
  7.2 72.4 %copy-start.7 = (bf16[2048,16]{0,1:T(8,128)(2,1)S(1)}, bf16[2048,16]{0,1:T(8,128)(2,1)}, u32[]{:S(2)}) copy-start(bf16[2048,16]{0,1:T(8,128)(2,1)} %param.26) | copy-start | bytes 196612
  7.2 90.5 %copy-start.4 = (bf16[2048,64]{0,1:T(8,128)(2,1)S(1)}, bf16[2048,64]{0,1:T(8,128)(2,1)}, u32[]{:S(2)}) copy-start(bf16[2048,64]{0,1:T(8,128)(2,1)} %param.24) | copy-start | bytes 786436
  7.2 57.3 %all-gather.4.cloned.1.call-start = ((), (), s32[]{:S(2)}) async-start(), calls=%async_computation.8 | async-start | bytes 1572864 | tf_op jit(solution)/shard_map/all_gather | solution.py:24
  51.1 65.0 %copy-start.5 = (bf16[2048,64]{0,1:T(8,128)(2,1)S(1)}, bf16[2048,64]{0,1:T(8,128)(2,1)}, u32[]{:S(2)}) copy-start(bf16[2048,64]{0,1:T(8,128)(2,1)} %param.23) | copy-start | bytes 786436
  65.8 67.5 %copy-start.2 = (bf16[8,3,3072]{2,0,1:T(8,128)(2,1)S(1)}, bf16[8,3,3072]{2,0,1:T(8,128)(2,1)}, u32[]{:S(2)}) copy-start(bf16[8,3,3072]{2,0,1:T(8,128)(2,1)} %param.32) | copy-start | bytes 442372
  66.9 25.4 %all-to-all-start.1 = ((bf16[32,8,16]{2,1,0:T(8,128)(2,1)}), bf16[32,8,16]{2,1,0:T(8,128)(2,1)S(1)}, u32[]{:S(2)}, u32[]{:S(2)}) async-start(bf16[32,8,16]{2,1,0:T(8,128)(2,1)} %bitcast.7), calls=%async_computation.1 | async-start | bytes 131072 | tf_op jit(solution)/shard_map/all_to_all | solution.py:135
  92.3 18.6 %all-to-all-start.2 = ((bf16[32,8,16]{2,1,0:T(8,128)(2,1)}), bf16[32,8,16]{2,1,0:T(8,128)(2,1)S(1)}, u32[]{:S(2)}, u32[]{:S(2)}) async-start(bf16[32,8,16]{2,1,0:T(8,128)(2,1)} %bitcast.9), calls=%async_computation.2 | async-start | bytes 131072 | tf_op jit(solution)/shard_map/all_to_all | solution.py:136
  110.9 17.0 %all-to-all-start = ((bf16[32,2,256]{2,1,0:T(2,128)(2,1)}), bf16[32,2,256]{2,1,0:T(2,128)(2,1)S(1)}, u32[]{:S(2)}, u32[]{:S(2)}) async-start(bf16[32,2,256]{2,1,0:T(2,128)(2,1)} %reshape.124), calls=%async_computation | async-start | bytes 65536 | tf_op jit(solution)/shard_map/all_to_all | solution.py:134
  127.9 16.9 %all-to-all-start.3 = ((bf16[32,2,256]{2,1,0:T(2,128)(2,1)}), bf16[32,2,256]{2,1,0:T(2,128)(2,1)S(1)}, u32[]{:S(2)}, u32[]{:S(2)}) async-start(bf16[32,2,256]{2,1,0:T(2,128)(2,1)} %reshape.126), calls=%async_computation.3 | async-start | bytes 65536 | tf_op jit(solution)/shard_map/all_to_all | solution.py:133
  150.6 3.4 copy-start.1
  154.0 23.2 %copy-start.8 = (bf16[2048]{0:T(1024)(128)(2,1)S(1)}, bf16[2048]{0:T(1024)(128)(2,1)}, u32[]{:S(2)}) copy-start(bf16[2048]{0:T(1024)(128)(2,1)} %param.36) | copy-start | bytes 12292
  154.0 23.2 %copy-start.9 = (s32[8,2]{0,1:T(2,128)S(1)}, s32[8,2]{0,1:T(2,128)}, u32[]{:S(2)}) copy-start(s32[8,2]{0,1:T(2,128)} %param.40) | copy-start | bytes 196
  154.0 77.2 %copy-start.3 = (bf16[8,2048]{1,0:T(8,128)(2,1)S(1)}, bf16[8,2048]{1,0:T(8,128)(2,1)}, u32[]{:S(2)}) copy-start(bf16[8,2048]{1,0:T(8,128)(2,1)} %param.21) | copy-start | bytes 98308
  172.0 59.0 %all-to-all-start.5 = ((bf16[32,8,2048]{2,1,0:T(8,128)(2,1)}), bf16[32,8,2048]{2,1,0:T(8,128)(2,1)S(1)}, u32[]{:S(2)}, u32[]{:S(2)}) async-start(bf16[32,8,2048]{2,1,0:T(8,128)(2,1)} %fusion.9), calls=%async_computation.5 | async-start | bytes 2097152 | tf_op jit(solution)/shard_map/all_to_all | solution.py:43
  231.0 60.5 %copy-start.11 = (bf16[2048,896]{1,0:T(8,128)(2,1)S(1)}, bf16[2048,896]{1,0:T(8,128)(2,1)}, u32[]{:S(2)}) copy-start(bf16[2048,896]{1,0:T(8,128)(2,1)} %param.37) | copy-start | bytes 11010052
  292.7 13.3 %copy-start.10 = (f32[8,2]{0,1:T(2,128)S(1)}, f32[8,2]{0,1:T(2,128)}, u32[]{:S(2)}) copy-start(f32[8,2]{0,1:T(2,128)} %param.41) | copy-start | bytes 196
  299.3 60.6 %all-to-all-start.7 = ((bf16[32,8,2048]{2,1,0:T(8,128)(2,1)}), bf16[32,8,2048]{2,1,0:T(8,128)(2,1)S(1)}, u32[]{:S(2)}, u32[]{:S(2)}) async-start(bf16[32,8,2048]{2,1,0:T(8,128)(2,1)} %fusion.6), calls=%async_computation.7 | async-start | bytes 2097152 | tf_op jit(solution)/shard_map/all_to_all | solution.py:176
Sparse Core Ops, SparseCore 0:
  51.3 13.1 all-gather.3
where the time goes:
time: 372 us; the launch traced here: 368 us
  waiting for transfers between devices  161 us (43%)
  blocking collectives  117 us (31%)
  starting transfers between devices  40.5 us (11%)
  matrix products  15.2 us (4%)
  between operations  14.4 us (4%)
  other arithmetic  11.6 us (3%)
  local copies, waits for them, and re-layouts  8.1 us (2%)
    all_to_all x1, blocking collectives, on_device(): lax.all_to_all(send_rows, EP, split_axis=0, concat_axis=0, tiled=True)  59.9 us
    all_to_all x1, waiting for transfers between devices, sum_at_owner(): lax.all_to_all(parts, axis, split_axis=0, concat_axis=0, tiled=True)  53.6 us
    all_to_all x1, waiting for transfers between devices, on_device(): lax.all_to_all(expert_out.astype(jnp.bfloat16), EP, split_axis=0, concat_...  53 us
    all_gather x1, blocking collectives, all_blocks(): parts = lax.all_gather(parts, axes[k])  41.3 us
    all_to_all x1, blocking collectives, on_device(): lax.all_to_all(gated, EP, split_axis=1, concat_axis=0, tiled=True)  16 us
    all_to_all x1, starting transfers between devices, on_device(): lax.all_to_all(write_cols, EP, split_axis=0, concat_axis=1, tiled=True)  12.7 us
    all_to_all x1, waiting for transfers between devices, on_device(): lax.all_to_all(read_cols, EP, split_axis=0, concat_axis=1, tiled=True)  11.9 us
    all_to_all x1, waiting for transfers between devices, on_device(): lax.all_to_all(write_cols, EP, split_axis=0, concat_axis=1, tiled=True)  11.5 us
  transfers between devices with their start and end apart: 7, of which 7 were waited for; matrix products, arithmetic and copies ran while one was open for 3% of the time, Pallas kernels for 0%

commit v1 on v0

v1 whole, which is shorter than its diff:
```python
import functools

import jax
import jax.numpy as jnp
from jax import lax
from jax.experimental import pallas as pl
from jax.experimental.pallas import tpu as pltpu
from jax.sharding import PartitionSpec as P

EXPERTS = 8
GRP_EP = ("grp", "ep")
MESH = pl.DeviceIdType.MESH
F32 = jnp.float32
BF16 = jnp.bfloat16
norm_eps = 1e-06

TREE = (((0, 3), (0, 1)), ((3, 6), (3, 4), (1, 2)), ((6, 8), (6, 7), (4, 5)))
EDGES = tuple(
    (sign, f, t) for phase in TREE for (f, t) in phase for sign in (1, -1) if not (t == 8 and sign < 0)
)
SLOT = {edge: k for k, edge in enumerate(EDGES)}
GREET = (1, -1, 2, -2, 3, -3)


def rms_scale(floats, gain):
    return floats * lax.rsqrt(jnp.mean(floats * floats, axis=-1, keepdims=True) + norm_eps) * gain


def nt_dot(a, b):
    return lax.dot_general(a, b, (((1,), (1,)), ((), ())), preferred_element_type=F32)


def step_kernel(
    chips,
    hidden_ref,
    norm_gain_ref,
    outgate_ref,
    input_ref,
    write_ref,
    read_ref,
    step_weight_ref,
    step_bias_ref,
    decay_log_ref,
    skip_gain_ref,
    conv_weight_ref,
    conv_state_ref,
    mixer_state_ref,
    inner_gain_ref,
    out_weight_ref,
    ffn_gain_ref,
    expert_gate_ref,
    expert_up_ref,
    expert_down_ref,
    ids_ref,
    route_ref,
    result_ref,
    new_state_ref,
    new_conv_ref,
    rows_a,
    rows_e,
    proj_w,
    out_w,
    gate_w,
    up_w,
    down_w,
    proj_send,
    proj_recv,
    head_send,
    head_recv,
    part32,
    part_send,
    part_recv,
    units,
    reps,
    conv_part,
    scaled_ref,
    maps_ref,
    rate_ref,
    weight_sem,
    pair_send,
    pair_recv,
    gather_send,
    gather_recv,
    swap_send,
    swap_recv,
    sum_send,
    sum_recv,
):
    seqs, width = hidden_ref.shape
    heads, head_dim, state_width = mixer_state_ref.shape[1:]
    groups = (conv_weight_ref.shape[1] - width) // (2 * state_width)
    per_group = heads // groups
    group_width = per_group * head_dim
    lanes = width // chips
    half = outgate_ref.shape[0]
    thin = write_ref.shape[0]
    hidden_units = expert_gate_ref.shape[1]
    ep = lax.axis_index("ep")
    chip, core = ep // 2, ep % 2

    def at(offset):
        return lax.rem(chip + offset + chips, chips)

    def dev(where):
        return {"ep": where * 2 + core}

    sibling = {"ep": chip * 2 + 1 - core}

    barrier = pltpu.get_barrier_semaphore()
    for offset in GREET:
        pl.semaphore_signal(barrier, inc=1, device_id=dev(at(offset)), device_id_type=MESH)
    pl.semaphore_signal(barrier, inc=1, device_id=sibling, device_id_type=MESH)

    def own_rows(buf, first, count):
        return buf.at[pl.ds(pl.multiple_of(first + count * core, count), count)]

    def own_cols(buf):
        return buf.at[:, pl.ds(pl.multiple_of(hidden_units * core, 128), hidden_units)]

    shards = (
        (outgate_ref, own_rows(proj_w, 0, half)),
        (input_ref, own_rows(proj_w, 2 * half, half)),
        (write_ref, own_rows(proj_w, 4 * half, thin)),
        (read_ref, own_rows(proj_w, 4 * half + 2 * thin, thin)),
        (out_weight_ref, own_rows(out_w, 0, half)),
        (expert_gate_ref, own_cols(gate_w)),
        (expert_up_ref, own_cols(up_w)),
        (expert_down_ref, own_rows(down_w, 0, hidden_units)),
    )
    local = [pltpu.make_async_copy(src, dst, weight_sem.at[k]) for k, (src, dst) in enumerate(shards)]
    local.append(pltpu.make_async_copy(mixer_state_ref, new_state_ref, weight_sem.at[len(shards)]))
    for k in (0, 1, 2, 3):
        local[k].start()

    hidden = hidden_ref[...].astype(F32)
    normed = rms_scale(hidden, norm_gain_ref[...].astype(F32)).astype(BF16)
    rows_a[chip] = normed
    pl.semaphore_wait(barrier, len(GREET) + 1)

    pair = [
        pltpu.make_async_remote_copy(
            src_ref=src, dst_ref=dst, send_sem=pair_send.at[k], recv_sem=pair_recv.at[k], device_id=sibling, device_id_type=MESH
        )
        for k, (src, dst) in enumerate(shards)
    ]

    def all_gather(buf, n):
        started, seen = [], set()

        def copy(edge, source, where):
            k = SLOT[edge]
            return pltpu.make_async_remote_copy(
                src_ref=buf.at[source],
                dst_ref=buf.at[source],
                send_sem=gather_send.at[n, k],
                recv_sem=gather_recv.at[n, k],
                device_id=dev(where),
                device_id_type=MESH,
            )

        def arrive(sign, offset):
            if offset and (sign, offset) not in seen:
                seen.add((sign, offset))
                (edge,) = [e for e in EDGES if e[0] == sign and e[2] == offset]
                copy(edge, at(-sign * offset), chip).wait_recv()

        for sign, f, t in EDGES:
            arrive(sign, f)
            c = copy((sign, f, t), at(-sign * f), at(sign * (t - f)))
            c.start()
            started.append(c)
            if (sign, f, t) == EDGES[3]:
                yield
        for sign, f, t in EDGES:
            arrive(sign, t)
        for c in started:
            c.wait_send()

    def swap(send, recv, n):
        copies = []
        for k in range(1, chips):
            offset = (k + 1) // 2 * (1 if k % 2 else -1)
            there = at(offset)
            copies.append(
                pltpu.make_async_remote_copy(
                    src_ref=send.at[there],
                    dst_ref=recv.at[chip],
                    send_sem=swap_send.at[n, k],
                    recv_sem=swap_recv.at[n, chip],
                    device_id=dev(there),
                    device_id_type=MESH,
                )
            )
        for c in copies[::-1]:
            c.start()

        def finish():
            for k in range(1, chips):
                there = at(k)
                pltpu.make_async_remote_copy(
                    src_ref=send.at[there],
                    dst_ref=recv.at[there],
                    send_sem=swap_send.at[n, 0],
                    recv_sem=swap_recv.at[n, there],
                    device_id=dev(there),
                    device_id_type=MESH,
                ).wait_recv()
            for c in copies:
                c.wait_send()

        return finish

    def sum_at_owner(n):
        started = []

        def copy(edge, block, where):
            k = SLOT[edge]
            return pltpu.make_async_remote_copy(
                src_ref=part_send.at[n, block],
                dst_ref=part_recv.at[n, k],
                send_sem=sum_send.at[n, k],
                recv_sem=sum_recv.at[n, k],
                device_id=dev(where),
                device_id_type=MESH,
            )

        def gathered(sign, f):
            total = part32[at(-sign * f)]
            for edge in EDGES[::-1]:
                if edge[0] == sign and edge[1] == f:
                    copy(edge, chip, chip).wait_recv()
                    total = total + part_recv[n, SLOT[edge]].astype(F32)
            return total

        inner = {(sign, f) for sign, f, _ in EDGES}
        leaves = [e for e in EDGES if (e[0], e[2]) not in inner]
        order = sorted(leaves, key=lambda e: -e[2])
        order += [(s, f, t) for s, f, t in EDGES[::-1] if (s, t) in inner]
        for sign, f, t in order:
            block = at(-sign * t)
            if (sign, t) in inner:
                part_send[n, block] = gathered(sign, t).astype(BF16)
            c = copy((sign, f, t), block, at(-sign * (t - f)))
            c.start()
            started.append(c)
        total = part32[chip]
        for sign in (1, -1):
            for edge in EDGES[::-1]:
                if edge[0] == sign and edge[1] == 0:
                    copy(edge, chip, chip).wait_recv()
                    total = total + part_recv[n, SLOT[edge]].astype(F32)
        return total, started

    gather = all_gather(rows_a, 0)
    next(gather)
    for k in (0, 1, 2, 3):
        pair[k].start()
    local[8].start()
    for k in (4, 5, 6, 7):
        local[k].start()
        pair[k].start()

    old = conv_state_ref[...]
    taps = conv_weight_ref[...].astype(F32)
    new_conv_ref[0] = old[1]
    new_conv_ref[1] = old[2]
    conv_part[...] = (
        old[0].astype(F32) * taps[0:1] + old[1].astype(F32) * taps[1:2] + old[2].astype(F32) * taps[2:3]
    )
    step_raw = nt_dot(normed, step_weight_ref[...]) + step_bias_ref[...]
    step = jnp.maximum(step_raw, 0.0) + jnp.log1p(jnp.exp(-jnp.abs(step_raw)))
    rate = jnp.exp(-step * jnp.exp(decay_log_ref[...]))
    rate_ref[...] = rate
    spread = (
        lax.broadcasted_iota(jnp.int32, (heads, width), 1) // head_dim == lax.broadcasted_iota(jnp.int32, (heads, width), 0)
    ).astype(F32)
    wide = jnp.concatenate([step, rate, jnp.broadcast_to(skip_gain_ref[...], step.shape)], axis=0)
    reps[...] = jnp.dot(wide, spread, precision=lax.Precision.HIGHEST, preferred_element_type=F32)
    eye = (
        lax.broadcasted_iota(jnp.int32, (seqs, seqs), 0) == lax.broadcasted_iota(jnp.int32, (seqs, seqs), 1)
    ).astype(F32)

    def turned(values):
        return lax.dot_general(
            eye, values, (((1,), (1,)), ((), ())), precision=lax.Precision.HIGHEST, preferred_element_type=F32
        )

    ids = turned(ids_ref[...].astype(F32))
    route = turned(route_ref[...])
    shared = chips // EXPERTS
    proj_w[4 * half + 4 * thin :] = jnp.zeros((proj_w.shape[0] - 4 * half - 4 * thin, width), BF16)

    for _ in gather:
        pass
    for k in (0, 1, 2, 3):
        local[k].wait()
        pair[k].wait()

    proj = nt_dot(rows_a[...].reshape(chips * seqs, width), proj_w[...])
    lane = lax.broadcasted_iota(jnp.int32, (seqs, 128), 1)
    for j in range(chips):
        block = proj[j * seqs : (j + 1) * seqs]
        mine = jnp.where(ids == (j // shared), route, 0.0)
        mine = jnp.sum(mine, axis=1, keepdims=True)
        high = mine.astype(BF16).astype(F32)
        tail = jnp.where(
            lane == 64, high, jnp.where(lane == 65, mine - high, block[:, 4 * half :])
        )
        proj_send[j, :, : 4 * half] = block[:, : 4 * half].astype(BF16)
        proj_send[j, :, 4 * half :] = tail.astype(BF16)
    proj_recv[chip] = proj_send[chip]
    swap(proj_send, proj_recv, 0)()

    maps = []
    for first in (0, 2 * thin):
        for g in range(groups):
            total = jnp.zeros((seqs, 128), F32)
            for i in range(4):
                piece = proj_recv[4 * g + i, :, 4 * half :].astype(F32)
                shift = (2 * thin * i - first) % 128
                if shift:
                    piece = pltpu.roll(piece, shift, 1)
                total = jnp.where((lane >= 2 * thin * i) & (lane < 2 * thin * (i + 1)), piece, total)
            maps.append(total)
    gate = jnp.concatenate([proj_recv[j, :, :lanes] for j in range(chips)], axis=1).astype(F32)
    new_row = jnp.concatenate(
        [proj_recv[j, :, lanes : 2 * lanes].astype(F32) for j in range(chips)] + maps, axis=1
    )
    new_conv_ref[2] = new_row.astype(BF16)
    conv = conv_part[...] + new_row * taps[3:4]
    conv = conv * jax.nn.sigmoid(conv)
    inputs = conv[:, :width]
    scaled = inputs * reps[:seqs]
    scaled_ref[...] = scaled
    maps_ref[...] = conv[:, width:]
    local[8].wait()

    row = lax.broadcasted_iota(jnp.int32, (seqs, 1), 0)
    gated_in = []
    for g in range(groups):
        write_map = conv[:, width + g * state_width : width + (g + 1) * state_width]
        first = width + (groups + g) * state_width
        read_map = conv[:, first : first + state_width]
        read = jnp.zeros((seqs, group_width), F32)
        for s in range(seqs):
            block = new_state_ref[s, g * per_group : (g + 1) * per_group].reshape(group_width, state_width)
            picked = jnp.where(row == s, read_map, 0.0).astype(BF16)
            read = read + nt_dot(picked, block.astype(BF16))
        cols = slice(g * group_width, (g + 1) * group_width)
        both = jnp.sum(write_map * read_map, axis=1, keepdims=True)
        read_out = reps[seqs : 2 * seqs, cols] * read + scaled[:, cols] * both + reps[2 * seqs :, cols] * inputs[:, cols]
        g_cols = gate[:, cols]
        gated_in.append(read_out * (g_cols * jax.nn.sigmoid(g_cols)))
    gated = rms_scale(jnp.concatenate(gated_in, axis=1), inner_gain_ref[...].astype(F32)).astype(BF16)
    for j in range(chips):
        head_send[j] = gated[:, j * lanes : (j + 1) * lanes]
    head_recv[chip] = head_send[chip]
    finish = swap(head_send, head_recv, 1)

    def update(s, carry):
        rates = jnp.broadcast_to(rate_ref[pl.ds(s, 1)], (state_width, heads)).T
        here = row == s
        for g in range(groups):
            x = scaled_ref[:, g * group_width : (g + 1) * group_width]
            m = jnp.where(here, maps_ref[:, g * state_width : (g + 1) * state_width], 0.0)
            xh, mh = x.astype(BF16), m.astype(BF16)
            xl, ml = (x - xh.astype(F32)).astype(BF16), (m - mh.astype(F32)).astype(BF16)
            outer = lax.dot_general(
                jnp.concatenate([xh, xh, xl], axis=0),
                jnp.concatenate([mh, ml, mh], axis=0),
                (((0,), (0,)), ((), ())),
                preferred_element_type=F32,
            ).reshape(per_group, head_dim, state_width)
            where = pl.ds(g * per_group, per_group)
            factor = rates[g * per_group : (g + 1) * per_group].reshape(per_group, 1, state_width)
            new_state_ref[s, where] = new_state_ref[s, where] * factor + outer
        return carry

    lax.fori_loop(0, seqs, update, 0)
    finish()
    local[4].wait()
    pair[4].wait()

    heads_here = head_recv[...].reshape(chips * seqs, lanes)
    mixed = jnp.dot(heads_here, out_w[...], preferred_element_type=F32).reshape(chips, seqs, width)
    part32[...] = mixed
    part_send[0] = mixed.astype(BF16)
    mixed_out, sums = sum_at_owner(0)
    residual = (hidden_ref[...].astype(F32) + mixed_out).astype(BF16)
    result_ref[...] = residual
    rows_e[chip] = rms_scale(residual.astype(F32), ffn_gain_ref[...].astype(F32)).astype(BF16)
    for _ in all_gather(rows_e, 1):
        pass
    for c in sums:
        c.wait_send()
    for k in (5, 6, 7):
        local[k].wait()
        pair[k].wait()

    tile = 256

    def unit_tile(i, carry):
        cols = pl.ds(pl.multiple_of(i * tile, tile), tile)
        tokens = rows_e[...].reshape(chips * seqs, width)
        g = jnp.dot(tokens, gate_w[:, cols], preferred_element_type=F32)
        u = jnp.dot(tokens, up_w[:, cols], preferred_element_type=F32)
        units[:, cols] = (g * jax.nn.sigmoid(g) * u).astype(BF16)
        return carry

    lax.fori_loop(0, units.shape[1] // tile, unit_tile, 0)
    tails = proj_recv[:, :, 4 * half :].astype(F32)
    combine = tails[:, :, 64:65] + tails[:, :, 65:66]

    def down_tile(i, carry):
        cols = pl.ds(pl.multiple_of(i * tile, tile), tile)
        out = jnp.dot(units[...], down_w[:, cols], preferred_element_type=F32)
        out = out.reshape(chips, seqs, tile) * combine
        part32[:, :, cols] = out
        part_send[1, :, :, cols] = out.astype(BF16)
        return carry

    lax.fori_loop(0, width // tile, down_tile, 0)
    moe_sum, sums = sum_at_owner(1)
    result_ref[...] = (result_ref[...].astype(F32) + moe_sum).astype(BF16)
    for c in sums:
        c.wait_send()


def solution(mesh):
    chips = mesh.shape["ep"] // 2

    def on_device(
        hidden,
        norm_gain,
        outgate_weight,
        input_weight,
        write_weight,
        read_weight,
        step_weight,
        step_bias,
        decay_log,
        skip_gain,
        conv_weight,
        conv_state,
        mixer_state,
        inner_gain,
        out_weight,
        ffn_gain,
        expert_gate,
        expert_up,
        expert_down,
        route_ids,
        route_weights,
    ):
        seqs, width = hidden.shape
        conv_dim = conv_weight.shape[1]
        hidden_units = expert_gate.shape[1]
        half, thin = outgate_weight.shape[1], write_weight.shape[1]
        proj_cols = -(-(4 * half + 4 * thin + 2) // 128) * 128
        lanes = width // chips
        operands = (
            (hidden, 0),
            (norm_gain.reshape(1, -1), 0),
            (outgate_weight.T, 1),
            (input_weight.T, 1),
            (write_weight.T, 1),
            (read_weight.T, 1),
            (step_weight.T, 0),
            (step_bias.reshape(1, -1), 0),
            (decay_log.reshape(1, -1), 0),
            (skip_gain.reshape(1, -1), 0),
            (conv_weight, 0),
            (conv_state.transpose(1, 0, 2), 0),
            (mixer_state, 1),
            (inner_gain.reshape(1, -1), 0),
            (out_weight, 1),
            (ffn_gain.reshape(1, -1), 0),
            (expert_gate, 1),
            (expert_up, 1),
            (expert_down, 1),
            (route_ids.T, 0),
            (route_weights.T, 0),
        )
        vmem = pl.BlockSpec(memory_space=pltpu.VMEM)
        hbm = pl.BlockSpec(memory_space=pltpu.HBM)
        edges = len(EDGES)
        result, new_state, new_conv = pl.pallas_call(
            functools.partial(step_kernel, chips),
            out_shape=(
                jax.ShapeDtypeStruct((seqs, width), BF16),
                pltpu.VMEM(mixer_state.shape, F32),
                jax.ShapeDtypeStruct((conv_state.shape[1], seqs, conv_dim), BF16),
            ),
            in_specs=[hbm if big else vmem for _, big in operands],
            out_specs=(vmem, vmem, vmem),
            scratch_shapes=[
                pltpu.VMEM((chips, seqs, width), BF16),
                pltpu.VMEM((chips, seqs, width), BF16),
                pltpu.VMEM((proj_cols, width), BF16),
                pltpu.VMEM((2 * half, width), BF16),
                pltpu.VMEM((width, 2 * hidden_units), BF16),
                pltpu.VMEM((width, 2 * hidden_units), BF16),
                pltpu.VMEM((2 * hidden_units, width), BF16),
                pltpu.VMEM((chips, seqs, proj_cols), BF16),
                pltpu.VMEM((chips, seqs, proj_cols), BF16),
                pltpu.VMEM((chips, seqs, lanes), BF16),
                pltpu.VMEM((chips, seqs, lanes), BF16),
                pltpu.VMEM((chips, seqs, width), F32),
                pltpu.VMEM((2, chips, seqs, width), BF16),
                pltpu.VMEM((2, edges, seqs, width), BF16),
                pltpu.VMEM((chips * seqs, 2 * hidden_units), BF16),
                pltpu.VMEM((3 * seqs, width), F32),
                pltpu.VMEM((seqs, conv_dim), F32),
                pltpu.VMEM((seqs, width), F32),
                pltpu.VMEM((seqs, conv_dim - width), F32),
                pltpu.VMEM((seqs, step_weight.shape[1]), F32),
                pltpu.SemaphoreType.DMA((9,)),
                pltpu.SemaphoreType.DMA((8,)),
                pltpu.SemaphoreType.DMA((8,)),
                pltpu.SemaphoreType.DMA((2, edges)),
                pltpu.SemaphoreType.DMA((2, edges)),
                pltpu.SemaphoreType.DMA((2, chips)),
                pltpu.SemaphoreType.DMA((2, chips)),
                pltpu.SemaphoreType.DMA((2, edges)),
                pltpu.SemaphoreType.DMA((2, edges)),
            ],
            compiler_params=pltpu.CompilerParams(
                collective_id=0, has_side_effects=True, vmem_limit_bytes=54 * 2**20
            ),
            name="step",
        )(*[value for value, _ in operands])
        return result, new_state, new_conv.transpose(1, 0, 2)

    return jax.shard_map(
        on_device,
        mesh=mesh,
        in_specs=(
            P(GRP_EP, None),
            P(),
            P(None, "ep"),
            P(None, "ep"),
            P(None, "ep"),
            P(None, "ep"),
            P(),
            P(),
            P(),
            P(),
            P(),
            P(GRP_EP, None, None),
            P(GRP_EP, None, None, None),
            P(),
            P("ep", None),
            P(),
            P(None, "ep"),
            P(None, "ep"),
            P("ep", None),
            P(GRP_EP, None),
            P(GRP_EP, None),
        ),
        out_specs=(P(GRP_EP, None), P(GRP_EP, None, None, None), P(GRP_EP, None, None)),
        check_vma=False,
    )
```

time: 372 us -> 107 us (0.29); the launches traced: 368 us -> 107 us
  waiting for transfers between devices: 161 us -> 0 us
  blocking collectives: 117 us -> 0 us
  Pallas kernels: 0 us -> 97.8 us
  starting transfers between devices: 40.5 us -> 0 us
  matrix products: 15.2 us -> 0 us
  between operations: 14.4 us -> 0.66 us
  other arithmetic: 11.6 us -> 0 us
    all_to_all x6 -> x0, waiting for transfers between devices: 151 us -> none  [the longest x1 53.6 us: sum_at_owner(): lax.all_to_all(parts, axis, split_axis=0, concat_axis=0, tiled=True)]
    pallas_call x0 -> x1, Pallas kernels: none -> 97.8 us  [on_device(): pl.pallas_call(functools.partial(step_kernel, chips), out_shape=(jax.Shap...]
    all_to_all x2 -> x0, blocking collectives: 76 us -> none  [the longest x1 59.9 us: on_device(): lax.all_to_all(send_rows, EP, split_axis=0, concat_axis=0, tiled=True)]
    all_gather x1 -> x0, blocking collectives: 41.3 us -> none  [all_blocks(): parts = lax.all_gather(parts, axes[k])]
    all_to_all x6 -> x0, starting transfers between devices: 40.4 us -> none  [the longest x1 12.7 us: on_device(): lax.all_to_all(write_cols, EP, split_axis=0, concat_axis=1, tiled=True)]
    dot_general x9 -> x0, matrix products: 15.2 us -> none  [the longest x1 6.52 us: on_device(): jnp.einsum('abf,fi->abi', units, expert_down, preferred_element_type=jnp....]
    all_gather x1 -> x0, waiting for transfers between devices: 9.15 us -> none  [all_blocks(): parts = lax.all_gather(parts, axes[k])]
    add x1 -> x0, other arithmetic: 5.5 us -> none  [mixer_step(): decay_rate[..., None, None] * old_state]
  transfers between devices with their start and end apart: 7 -> 0, of which waited for: 7 -> 0; matrix products, arithmetic and copies ran while one was open for 3% -> 0% of each run, Pallas kernels for 0% -> 0%
where the time goes in v1:
time: 107 us
  Pallas kernels  97.8 us (91%)
  local copies, waits for them, and re-layouts  8.55 us (8%)
    pallas_call x1, Pallas kernels, on_device(): pl.pallas_call(functools.partial(step_kernel, chips), out_shape=(jax.Shap...  97.8 us
    unnamed x7, local copies, waits for them, and re-layouts  4.68 us

profile of v1, /device:TPU:196, one launch (start us, length us, event | category | flops | bytes accessed | tf_op | source)
XLA Modules:
  0.0 107.0 jit_solution(3902520482347237765)
XLA Ops:
  0.6 1.3 %reshape.24.norm_gain_ref = bf16[1,2048]{1,0:T(2,128)(2,1)} reshape(bf16[2048]{0:T(1024)(128)(2,1)} %param.22) | data formatting | bytes 8192 | tf_op jit(solution)/shard_map/reshape | solution.py:463
  1.9 1.3 %reshape.28.inner_gain_ref = bf16[1,2048]{1,0:T(2,128)(2,1)} reshape(bf16[2048]{0:T(1024)(128)(2,1)} %param.34) | data formatting | bytes 8192 | tf_op jit(solution)/shard_map/reshape | solution.py:475
  3.2 1.3 %reshape.29.ffn_gain_ref = bf16[1,2048]{1,0:T(2,128)(2,1)} reshape(bf16[2048]{0:T(1024)(128)(2,1)} %param.36) | data formatting | bytes 8192 | tf_op jit(solution)/shard_map/reshape | solution.py:477
  4.5 97.8 %step.1 = (bf16[8,2048]{1,0:T(8,128)(2,1)}, f32[8,32,64,128]{3,2,1,0:T(8,128)S(1)}, bf16[3,8,3072]{2,1,0:T(8,128)(2,1)}) custom-call(bf16[8,2048]{1,0:T(8,128)(2,1)} %hidden_ref.1, bf16[1,2048]{1,0:T(2,128)(2,1)} %reshape.24.norm_gain_ref, bf16[64,2048]{1,0:T(8,128)(2,1)} %bitcast.12, bf16[64,2048]{1,0:T(8,128)(2,1)} %bitcast.13, bf16[16,2048]{1,0:T(8,128)(2,1)} %bitcast.17, ...), custom_call_target="tpu_custom_call" | custom-call | tf_op jit(solution)/shard_map/step/pallas_call | solution.py:487
  102.3 0.0 copy-start.1
  102.3 0.0 copy-start
  102.3 3.4 %copy.27 = f32[8,32,64,128]{3,2,1,0:T(8,128)} copy(f32[8,32,64,128]{3,2,1,0:T(8,128)S(1)} %get-tuple-element.10) | data formatting | bytes 16777216
  105.7 0.0 copy-done.1
  105.7 0.6 copy.28
  106.3 0.0 copy-done
  106.3 0.7 copy.29
Async XLA Ops:
  102.3 3.4 %copy-start.1 = (bf16[8,2048]{1,0:T(8,128)(2,1)S(1)}, bf16[8,2048]{1,0:T(8,128)(2,1)}, u32[]{:S(2)}) copy-start(bf16[8,2048]{1,0:T(8,128)(2,1)} %get-tuple-element.15) | copy-start | bytes 98308
  102.3 4.0 %copy-start = (bf16[3,8,3072]{2,1,0:T(8,128)(2,1)S(1)}, bf16[3,8,3072]{2,1,0:T(8,128)(2,1)}, u32[]{:S(2)}) copy-start(bf16[3,8,3072]{2,1,0:T(8,128)(2,1)} %get-tuple-element.8) | copy-start | bytes 442372

commit v2 on v1

--- a/solution.py
+++ b/solution.py
@@ -14,16 +14,22 @@
 BF16 = jnp.bfloat16
 norm_eps = 1e-06
 
-TREE = (((0, 3), (0, 1)), ((3, 6), (3, 4), (1, 2)), ((6, 8), (6, 7), (4, 5)))
-EDGES = tuple(
-    (sign, f, t) for phase in TREE for (f, t) in phase for sign in (1, -1) if not (t == 8 and sign < 0)
-)
-SLOT = {edge: k for k, edge in enumerate(EDGES)}
-GREET = (1, -1, 2, -2, 3, -3)
+def both_ways(*edges):
+    return tuple((sign, f, t) for (f, t) in edges for sign in (1, -1) if not (t == 8 and sign < 0))
+
+
+A16 = both_ways((0, 5), (0, 2), (0, 1), (5, 8), (5, 7), (5, 6), (5, 4), (2, 3))
+T13 = both_ways((0, 3), (0, 1), (3, 6), (3, 4), (1, 2), (6, 8), (6, 7), (4, 5))
+TREES = (A16, T13)
+GREET = sorted({way * abs(t - f) for tree in TREES for _, f, t in tree for way in (1, -1)})
 
 
 def rms_scale(floats, gain):
     return floats * lax.rsqrt(jnp.mean(floats * floats, axis=-1, keepdims=True) + norm_eps) * gain
+
+
+def row_of(vector_ref):
+    return vector_ref[...].astype(F32).reshape(1, -1)
 
 
 def nt_dot(a, b):
@@ -76,6 +82,20 @@
     scaled_ref,
     maps_ref,
     rate_ref,
+    total_ref,
+    hidden_buf,
+    norm_gain_buf,
+    step_weight_buf,
+    step_bias_buf,
+    decay_log_buf,
+    skip_gain_buf,
+    conv_weight_buf,
+    conv_state_buf,
+    inner_gain_buf,
+    ffn_gain_buf,
+    ids_buf,
+    route_buf,
+    small_sem,
     weight_sem,
     pair_send,
     pair_recv,
@@ -111,6 +131,24 @@
         pl.semaphore_signal(barrier, inc=1, device_id=dev(at(offset)), device_id_type=MESH)
     pl.semaphore_signal(barrier, inc=1, device_id=sibling, device_id_type=MESH)
 
+    smalls = (
+        (hidden_ref, hidden_buf),
+        (norm_gain_ref, norm_gain_buf),
+        (step_weight_ref, step_weight_buf),
+        (step_bias_ref, step_bias_buf),
+        (decay_log_ref, decay_log_buf),
+        (skip_gain_ref, skip_gain_buf),
+        (conv_weight_ref, conv_weight_buf),
+        (conv_state_ref, conv_state_buf),
+        (inner_gain_ref, inner_gain_buf),
+        (ffn_gain_ref, ffn_gain_buf),
+        (ids_ref, ids_buf),
+        (route_ref, route_buf),
+    )
+    small = [pltpu.make_async_copy(src, dst, small_sem.at[k]) for k, (src, dst) in enumerate(smalls)]
+    for c in small:
+        c.start()
+
     def own_rows(buf, first, count):
         return buf.at[pl.ds(pl.multiple_of(first + count * core, count), count)]
 
@@ -132,8 +170,9 @@
     for k in (0, 1, 2, 3):
         local[k].start()
 
-    hidden = hidden_ref[...].astype(F32)
-    normed = rms_scale(hidden, norm_gain_ref[...].astype(F32)).astype(BF16)
+    small[0].wait()
+    small[1].wait()
+    normed = rms_scale(hidden_buf[...].astype(F32), row_of(norm_gain_buf)).astype(BF16)
     rows_a[chip] = normed
     pl.semaphore_wait(barrier, len(GREET) + 1)
 
@@ -144,37 +183,46 @@
         for k, (src, dst) in enumerate(shards)
     ]
 
-    def all_gather(buf, n):
-        started, seen = [], set()
-
-        def copy(edge, source, where):
-            k = SLOT[edge]
-            return pltpu.make_async_remote_copy(
-                src_ref=buf.at[source],
-                dst_ref=buf.at[source],
-                send_sem=gather_send.at[n, k],
-                recv_sem=gather_recv.at[n, k],
-                device_id=dev(where),
-                device_id_type=MESH,
-            )
+    def by_core(work):
+        if TREES[0] == TREES[1]:
+            work(TREES[0])
+        else:
+            for k, tree in enumerate(TREES):
+                pl.when(core == k)(functools.partial(work, tree))
+
+    def block_copy(buf, n, tree, edge, source, where):
+        k = tree.index(edge)
+        return pltpu.make_async_remote_copy(
+            src_ref=buf.at[source],
+            dst_ref=buf.at[source],
+            send_sem=gather_send.at[n, k],
+            recv_sem=gather_recv.at[n, k],
+            device_id=dev(where),
+            device_id_type=MESH,
+        )
+
+    def gather_start(buf, n, tree):
+        for sign, f, t in tree:
+            if f == 0:
+                block_copy(buf, n, tree, (sign, f, t), chip, at(sign * t)).start()
+
+    def gather_finish(buf, n, tree):
+        seen = set()
 
         def arrive(sign, offset):
-            if offset and (sign, offset) not in seen:
+            if (sign, offset) not in seen:
                 seen.add((sign, offset))
-                (edge,) = [e for e in EDGES if e[0] == sign and e[2] == offset]
-                copy(edge, at(-sign * offset), chip).wait_recv()
-
-        for sign, f, t in EDGES:
-            arrive(sign, f)
-            c = copy((sign, f, t), at(-sign * f), at(sign * (t - f)))
-            c.start()
-            started.append(c)
-            if (sign, f, t) == EDGES[3]:
-                yield
-        for sign, f, t in EDGES:
+                (edge,) = [e for e in tree if e[0] == sign and e[2] == offset]
+                block_copy(buf, n, tree, edge, at(-sign * offset), chip).wait_recv()
+
+        for sign, f, t in tree:
+            if f:
+                arrive(sign, f)
+                block_copy(buf, n, tree, (sign, f, t), at(-sign * f), at(sign * (t - f))).start()
+        for sign, f, t in tree:
             arrive(sign, t)
-        for c in started:
-            c.wait_send()
+        for edge in tree:
+            block_copy(buf, n, tree, edge, chip, chip).wait_send()
 
     def swap(send, recv, n):
         copies = []
@@ -210,49 +258,41 @@
 
         return finish
 
-    def sum_at_owner(n):
-        started = []
-
-        def copy(edge, block, where):
-            k = SLOT[edge]
-            return pltpu.make_async_remote_copy(
-                src_ref=part_send.at[n, block],
-                dst_ref=part_recv.at[n, k],
-                send_sem=sum_send.at[n, k],
-                recv_sem=sum_recv.at[n, k],
-                device_id=dev(where),
-                device_id_type=MESH,
-            )
-
-        def gathered(sign, f):
-            total = part32[at(-sign * f)]
-            for edge in EDGES[::-1]:
+    def part_copy(n, tree, edge, block, where):
+        k = tree.index(edge)
+        return pltpu.make_async_remote_copy(
+            src_ref=part_send.at[n, block],
+            dst_ref=part_recv.at[n, k],
+            send_sem=sum_send.at[n, k],
+            recv_sem=sum_recv.at[n, k],
+            device_id=dev(where),
+            device_id_type=MESH,
+        )
+
+    def sum_at_owner(n, tree):
+        def with_arrived(total, sign, f):
+            for edge in tree:
                 if edge[0] == sign and edge[1] == f:
-                    copy(edge, chip, chip).wait_recv()
-                    total = total + part_recv[n, SLOT[edge]].astype(F32)
+                    part_copy(n, tree, edge, chip, chip).wait_recv()
+                    total = total + part_recv[n, tree.index(edge)].astype(F32)
             return total
 
-        inner = {(sign, f) for sign, f, _ in EDGES}
-        leaves = [e for e in EDGES if (e[0], e[2]) not in inner]
-        order = sorted(leaves, key=lambda e: -e[2])
-        order += [(s, f, t) for s, f, t in EDGES[::-1] if (s, t) in inner]
-        for sign, f, t in order:
+        inner = {(sign, f) for sign, f, _ in tree}
+        far = [e for e in tree if (e[0], e[2]) not in inner and e[1]]
+        near = [e for e in tree if (e[0], e[2]) not in inner and not e[1]]
+        for sign, f, t in far + [e for e in tree[::-1] if (e[0], e[2]) in inner] + near:
             block = at(-sign * t)
             if (sign, t) in inner:
-                part_send[n, block] = gathered(sign, t).astype(BF16)
-            c = copy((sign, f, t), block, at(-sign * (t - f)))
-            c.start()
-            started.append(c)
+                part_send[n, block] = with_arrived(part32[block], sign, t).astype(BF16)
+            part_copy(n, tree, (sign, f, t), block, at(-sign * (t - f))).start()
         total = part32[chip]
         for sign in (1, -1):
-            for edge in EDGES[::-1]:
-                if edge[0] == sign and edge[1] == 0:
-                    copy(edge, chip, chip).wait_recv()
-                    total = total + part_recv[n, SLOT[edge]].astype(F32)
-        return total, started
-
-    gather = all_gather(rows_a, 0)
-    next(gather)
+            total = with_arrived(total, sign, 0)
+        total_ref[...] = total
+        for edge in tree:
+            part_copy(n, tree, edge, chip, chip).wait_send()
+
+    by_core(functools.partial(gather_start, rows_a, 0))
     for k in (0, 1, 2, 3):
         pair[k].start()
     local[8].start()
@@ -260,21 +300,23 @@
         local[k].start()
         pair[k].start()
 
-    old = conv_state_ref[...]
-    taps = conv_weight_ref[...].astype(F32)
+    for c in small[2:]:
+        c.wait()
+    old = conv_state_buf[...]
+    taps = conv_weight_buf[...].astype(F32)
     new_conv_ref[0] = old[1]
     new_conv_ref[1] = old[2]
     conv_part[...] = (
         old[0].astype(F32) * taps[0:1] + old[1].astype(F32) * taps[1:2] + old[2].astype(F32) * taps[2:3]
     )
-    step_raw = nt_dot(normed, step_weight_ref[...]) + step_bias_ref[...]
+    step_raw = nt_dot(normed, step_weight_buf[...]) + step_bias_buf[...]
     step = jnp.maximum(step_raw, 0.0) + jnp.log1p(jnp.exp(-jnp.abs(step_raw)))
-    rate = jnp.exp(-step * jnp.exp(decay_log_ref[...]))
+    rate = jnp.exp(-step * jnp.exp(decay_log_buf[...]))
     rate_ref[...] = rate
     spread = (
         lax.broadcasted_iota(jnp.int32, (heads, width), 1) // head_dim == lax.broadcasted_iota(jnp.int32, (heads, width), 0)
     ).astype(F32)
-    wide = jnp.concatenate([step, rate, jnp.broadcast_to(skip_gain_ref[...], step.shape)], axis=0)
+    wide = jnp.concatenate([step, rate, jnp.broadcast_to(skip_gain_buf[...], step.shape)], axis=0)
     reps[...] = jnp.dot(wide, spread, precision=lax.Precision.HIGHEST, preferred_element_type=F32)
     eye = (
         lax.broadcasted_iota(jnp.int32, (seqs, seqs), 0) == lax.broadcasted_iota(jnp.int32, (seqs, seqs), 1)
@@ -285,13 +327,12 @@
             eye, values, (((1,), (1,)), ((), ())), precision=lax.Precision.HIGHEST, preferred_element_type=F32
         )
 
-    ids = turned(ids_ref[...].astype(F32))
-    route = turned(route_ref[...])
+    ids = turned(ids_buf[...].astype(F32))
+    route = turned(route_buf[...])
     shared = chips // EXPERTS
     proj_w[4 * half + 4 * thin :] = jnp.zeros((proj_w.shape[0] - 4 * half - 4 * thin, width), BF16)
 
-    for _ in gather:
-        pass
+    by_core(functools.partial(gather_finish, rows_a, 0))
     for k in (0, 1, 2, 3):
         local[k].wait()
         pair[k].wait()
@@ -351,7 +392,7 @@
         read_out = reps[seqs : 2 * seqs, cols] * read + scaled[:, cols] * both + reps[2 * seqs :, cols] * inputs[:, cols]
         g_cols = gate[:, cols]
         gated_in.append(read_out * (g_cols * jax.nn.sigmoid(g_cols)))
-    gated = rms_scale(jnp.concatenate(gated_in, axis=1), inner_gain_ref[...].astype(F32)).astype(BF16)
+    gated = rms_scale(jnp.concatenate(gated_in, axis=1), row_of(inner_gain_buf)).astype(BF16)
     for j in range(chips):
         head_send[j] = gated[:, j * lanes : (j + 1) * lanes]
     head_recv[chip] = head_send[chip]
@@ -385,14 +426,12 @@
     mixed = jnp.dot(heads_here, out_w[...], preferred_element_type=F32).reshape(chips, seqs, width)
     part32[...] = mixed
     part_send[0] = mixed.astype(BF16)
-    mixed_out, sums = sum_at_owner(0)
-    residual = (hidden_ref[...].astype(F32) + mixed_out).astype(BF16)
+    by_core(functools.partial(sum_at_owner, 0))
+    residual = (hidden_buf[...].astype(F32) + total_ref[...]).astype(BF16)
     result_ref[...] = residual
-    rows_e[chip] = rms_scale(residual.astype(F32), ffn_gain_ref[...].astype(F32)).astype(BF16)
-    for _ in all_gather(rows_e, 1):
-        pass
-    for c in sums:
-        c.wait_send()
+    rows_e[chip] = rms_scale(residual.astype(F32), row_of(ffn_gain_buf)).astype(BF16)
+    by_core(functools.partial(gather_start, rows_e, 1))
+    by_core(functools.partial(gather_finish, rows_e, 1))
     for k in (5, 6, 7):
         local[k].wait()
         pair[k].wait()
@@ -407,7 +446,7 @@
         units[:, cols] = (g * jax.nn.sigmoid(g) * u).astype(BF16)
         return carry
 
-    lax.fori_loop(0, units.shape[1] // tile, unit_tile, 0)
+    lax.fori_loop(0, units.shape[1] // tile, unit_tile, 0, unroll=True)
     tails = proj_recv[:, :, 4 * half :].astype(F32)
     combine = tails[:, :, 64:65] + tails[:, :, 65:66]
 
@@ -419,11 +458,9 @@
         part_send[1, :, :, cols] = out.astype(BF16)
         return carry
 
-    lax.fori_loop(0, width // tile, down_tile, 0)
-    moe_sum, sums = sum_at_owner(1)
-    result_ref[...] = (result_ref[...].astype(F32) + moe_sum).astype(BF16)
-    for c in sums:
-        c.wait_send()
+    lax.fori_loop(0, width // tile, down_tile, 0, unroll=True)
+    by_core(functools.partial(sum_at_owner, 1))
+    result_ref[...] = (result_ref[...].astype(F32) + total_ref[...]).astype(BF16)
 
 
 def solution(mesh):
@@ -459,39 +496,40 @@
         proj_cols = -(-(4 * half + 4 * thin + 2) // 128) * 128
         lanes = width // chips
         operands = (
-            (hidden, 0),
-            (norm_gain.reshape(1, -1), 0),
-            (outgate_weight.T, 1),
-            (input_weight.T, 1),
-            (write_weight.T, 1),
-            (read_weight.T, 1),
-            (step_weight.T, 0),
-            (step_bias.reshape(1, -1), 0),
-            (decay_log.reshape(1, -1), 0),
-            (skip_gain.reshape(1, -1), 0),
-            (conv_weight, 0),
-            (conv_state.transpose(1, 0, 2), 0),
-            (mixer_state, 1),
-            (inner_gain.reshape(1, -1), 0),
-            (out_weight, 1),
-            (ffn_gain.reshape(1, -1), 0),
-            (expert_gate, 1),
-            (expert_up, 1),
-            (expert_down, 1),
-            (route_ids.T, 0),
-            (route_weights.T, 0),
+            hidden,
+            norm_gain,
+            outgate_weight.T,
+            input_weight.T,
+            write_weight.T,
+            read_weight.T,
+            step_weight.T,
+            step_bias.reshape(1, -1),
+            decay_log.reshape(1, -1),
+            skip_gain.reshape(1, -1),
+            conv_weight,
+            conv_state.transpose(1, 0, 2),
+            mixer_state,
+            inner_gain,
+            out_weight,
+            ffn_gain,
+            expert_gate,
+            expert_up,
+            expert_down,
+            route_ids.T,
+            route_weights.T,
         )
         vmem = pl.BlockSpec(memory_space=pltpu.VMEM)
-        hbm = pl.BlockSpec(memory_space=pltpu.HBM)
-        edges = len(EDGES)
+        hbm = pl.BlockSpec(memory_space=pl.ANY)
+        smalls = [operands[k] for k in (0, 1, 6, 7, 8, 9, 10, 11, 13, 15, 19, 20)]
+        edges = len(TREES[0])
         result, new_state, new_conv = pl.pallas_call(
             functools.partial(step_kernel, chips),
             out_shape=(
-                jax.ShapeDtypeStruct((seqs, width), BF16),
+                pltpu.VMEM((seqs, width), BF16),
                 pltpu.VMEM(mixer_state.shape, F32),
-                jax.ShapeDtypeStruct((conv_state.shape[1], seqs, conv_dim), BF16),
+                pltpu.VMEM((conv_state.shape[1], seqs, conv_dim), BF16),
             ),
-            in_specs=[hbm if big else vmem for _, big in operands],
+            in_specs=[hbm] * len(operands),
             out_specs=(vmem, vmem, vmem),
             scratch_shapes=[
                 pltpu.VMEM((chips, seqs, width), BF16),
@@ -514,6 +552,9 @@
                 pltpu.VMEM((seqs, width), F32),
                 pltpu.VMEM((seqs, conv_dim - width), F32),
                 pltpu.VMEM((seqs, step_weight.shape[1]), F32),
+                pltpu.VMEM((seqs, width), F32),
+                *[pltpu.VMEM(value.shape, value.dtype) for value in smalls],
+                pltpu.SemaphoreType.DMA((len(smalls),)),
                 pltpu.SemaphoreType.DMA((9,)),
                 pltpu.SemaphoreType.DMA((8,)),
                 pltpu.SemaphoreType.DMA((8,)),
@@ -528,7 +569,7 @@
                 collective_id=0, has_side_effects=True, vmem_limit_bytes=54 * 2**20
             ),
             name="step",
-        )(*[value for value, _ in operands])
+        )(*operands)
         return result, new_state, new_conv.transpose(1, 0, 2)
 
     return jax.shard_map(

time: 107 us -> 96.6 us (0.903); the launches traced: 107 us -> 94.8 us
  Pallas kernels: 97.8 us -> 89.4 us
  local copies, waits for them, and re-layouts: 8.55 us -> 4.67 us
    pallas_call x1, Pallas kernels: 97.8 us -> 89.4 us  [on_device(): pl.pallas_call(functools.partial(step_kernel, chips), out_shape=(pltpu.VM...]
    reshape x3 -> x0, local copies, waits for them, and re-layouts: 3.87 us -> none  [the longest x1 1.29 us: on_device(): norm_gain.reshape(1, -1)]
    unnamed x7 -> x3, local copies, waits for them, and re-layouts: 4.68 us -> 4.67 us
where the time goes in v2:
time: 96.6 us; the launch traced here: 94.8 us
  Pallas kernels  89.4 us (93%)
  local copies, waits for them, and re-layouts  4.67 us (5%)
    pallas_call x1, Pallas kernels, on_device(): pl.pallas_call(functools.partial(step_kernel, chips), out_shape=(pltpu.VM...  89.4 us
    unnamed x3, local copies, waits for them, and re-layouts  4.67 us

profile of v2, /device:TPU:196, one launch (start us, length us, event | category | flops | bytes accessed | tf_op | source)
XLA Modules:
  0.0 94.8 jit_solution(4384477281788675135)
XLA Ops:
  0.6 89.4 %step.1 = (bf16[8,2048]{1,0:T(8,128)(2,1)S(1)}, f32[8,32,64,128]{3,2,1,0:T(8,128)S(1)}, bf16[3,8,3072]{2,1,0:T(8,128)(2,1)S(1)}) custom-call(bf16[8,2048]{1,0:T(8,128)(2,1)} %hidden_ref.1, bf16[2048]{0:T(1024)(128)(2,1)} %norm_gain_ref.1, bf16[64,2048]{1,0:T(8,128)(2,1)} %bitcast.13, bf16[64,2048]{1,0:T(8,128)(2,1)} %bitcast.14, bf16[16,2048]{1,0:T(8,128)(2,1)} %bitcast.17, ...), custom_call_target="tpu_custom_call" | custom-call | tf_op jit(solution)/shard_map/step/pallas_call | solution.py:525
  90.1 0.6 copy.27
  90.7 0.7 copy.29
  91.4 3.4 %copy.28 = f32[8,32,64,128]{3,2,1,0:T(8,128)} copy(f32[8,32,64,128]{3,2,1,0:T(8,128)S(1)} %get-tuple-element.10) | data formatting | bytes 16777216

commit v3 on v2

--- a/solution.py
+++ b/solution.py
@@ -20,8 +20,8 @@
 
 A16 = both_ways((0, 5), (0, 2), (0, 1), (5, 8), (5, 7), (5, 6), (5, 4), (2, 3))
 T13 = both_ways((0, 3), (0, 1), (3, 6), (3, 4), (1, 2), (6, 8), (6, 7), (4, 5))
-TREES = (A16, T13)
-GREET = sorted({way * abs(t - f) for tree in TREES for _, f, t in tree for way in (1, -1)})
+TREES = ((A16, T13), (A16, T13), (A16, T13), (A16, T13))
+GREET = sorted({way * abs(t - f) for pair in TREES for tree in pair for _, f, t in tree for way in (1, -1)})
 
 
 def rms_scale(floats, gain):
@@ -83,6 +83,7 @@
     maps_ref,
     rate_ref,
     total_ref,
+    state16,
     hidden_buf,
     norm_gain_buf,
     step_weight_buf,
@@ -183,12 +184,9 @@
         for k, (src, dst) in enumerate(shards)
     ]
 
-    def by_core(work):
-        if TREES[0] == TREES[1]:
-            work(TREES[0])
-        else:
-            for k, tree in enumerate(TREES):
-                pl.when(core == k)(functools.partial(work, tree))
+    def by_core(exchange, work):
+        for k, tree in enumerate(TREES[exchange]):
+            pl.when(core == k)(functools.partial(work, tree))
 
     def block_copy(buf, n, tree, edge, source, where):
         k = tree.index(edge)
@@ -206,57 +204,55 @@
             if f == 0:
                 block_copy(buf, n, tree, (sign, f, t), chip, at(sign * t)).start()
 
-    def gather_finish(buf, n, tree):
+    def gather_arrived(buf, n, tree, arrivals):
+        for sign, offset in arrivals:
+            (edge,) = [e for e in tree if e[0] == sign and e[2] == offset]
+            block_copy(buf, n, tree, edge, at(-sign * offset), chip).wait_recv()
+
+    def first_arrivals(tree):
+        return [(s, f) for s, f, t in tree if f] + [(s, t) for s, f, t in tree if not f]
+
+    def gather_relay(buf, n, tree):
         seen = set()
-
-        def arrive(sign, offset):
-            if (sign, offset) not in seen:
-                seen.add((sign, offset))
-                (edge,) = [e for e in tree if e[0] == sign and e[2] == offset]
-                block_copy(buf, n, tree, edge, at(-sign * offset), chip).wait_recv()
-
         for sign, f, t in tree:
             if f:
-                arrive(sign, f)
+                if (sign, f) not in seen:
+                    seen.add((sign, f))
+                    gather_arrived(buf, n, tree, [(sign, f)])
                 block_copy(buf, n, tree, (sign, f, t), at(-sign * f), at(sign * (t - f))).start()
-        for sign, f, t in tree:
-            arrive(sign, t)
+        gather_arrived(buf, n, tree, [a for a in dict.fromkeys(first_arrivals(tree)) if a not in seen])
+
+    def gather_last(buf, n, tree):
+        first = first_arrivals(tree)
+        gather_arrived(buf, n, tree, [(s, t) for s, f, t in tree if (s, t) not in first])
+
+    def gather_sent(buf, n, tree):
         for edge in tree:
             block_copy(buf, n, tree, edge, chip, chip).wait_send()
 
-    def swap(send, recv, n):
-        copies = []
+    def swap_copy(send, recv, n, there):
+        return pltpu.make_async_remote_copy(
+            src_ref=send.at[there],
+            dst_ref=recv.at[chip],
+            send_sem=swap_send.at[n, there],
+            recv_sem=swap_recv.at[n, chip],
+            device_id=dev(there),
+            device_id_type=MESH,
+        )
+
+    def swap_finish(send, recv, n):
         for k in range(1, chips):
-            offset = (k + 1) // 2 * (1 if k % 2 else -1)
-            there = at(offset)
-            copies.append(
-                pltpu.make_async_remote_copy(
-                    src_ref=send.at[there],
-                    dst_ref=recv.at[chip],
-                    send_sem=swap_send.at[n, k],
-                    recv_sem=swap_recv.at[n, chip],
-                    device_id=dev(there),
-                    device_id_type=MESH,
-                )
-            )
-        for c in copies[::-1]:
-            c.start()
-
-        def finish():
-            for k in range(1, chips):
-                there = at(k)
-                pltpu.make_async_remote_copy(
-                    src_ref=send.at[there],
-                    dst_ref=recv.at[there],
-                    send_sem=swap_send.at[n, 0],
-                    recv_sem=swap_recv.at[n, there],
-                    device_id=dev(there),
-                    device_id_type=MESH,
-                ).wait_recv()
-            for c in copies:
-                c.wait_send()
-
-        return finish
+            there = at(k)
+            pltpu.make_async_remote_copy(
+                src_ref=send.at[there],
+                dst_ref=recv.at[there],
+                send_sem=swap_send.at[n, there],
+                recv_sem=swap_recv.at[n, there],
+                device_id=dev(there),
+                device_id_type=MESH,
+            ).wait_recv()
+        for k in range(1, chips):
+            swap_copy(send, recv, n, at(k)).wait_send()
 
     def part_copy(n, tree, edge, block, where):
         k = tree.index(edge)
@@ -292,7 +288,7 @@
         for edge in tree:
             part_copy(n, tree, edge, chip, chip).wait_send()
 
-    by_core(functools.partial(gather_start, rows_a, 0))
+    by_core(0, functools.partial(gather_start, rows_a, 0))
     for k in (0, 1, 2, 3):
         pair[k].start()
     local[8].start()
@@ -332,25 +328,48 @@
     shared = chips // EXPERTS
     proj_w[4 * half + 4 * thin :] = jnp.zeros((proj_w.shape[0] - 4 * half - 4 * thin, width), BF16)
 
-    by_core(functools.partial(gather_finish, rows_a, 0))
-    for k in (0, 1, 2, 3):
-        local[k].wait()
-        pair[k].wait()
-
-    proj = nt_dot(rows_a[...].reshape(chips * seqs, width), proj_w[...])
     lane = lax.broadcasted_iota(jnp.int32, (seqs, 128), 1)
-    for j in range(chips):
-        block = proj[j * seqs : (j + 1) * seqs]
-        mine = jnp.where(ids == (j // shared), route, 0.0)
-        mine = jnp.sum(mine, axis=1, keepdims=True)
-        high = mine.astype(BF16).astype(F32)
-        tail = jnp.where(
-            lane == 64, high, jnp.where(lane == 65, mine - high, block[:, 4 * half :])
-        )
-        proj_send[j, :, : 4 * half] = block[:, : 4 * half].astype(BF16)
-        proj_send[j, :, 4 * half :] = tail.astype(BF16)
+
+    def project(offsets):
+        there = [at(offset) for offset in offsets]
+        rows = jnp.concatenate([rows_a[j] for j in there], axis=0)
+        proj = nt_dot(rows, proj_w[...])
+        for k, j in enumerate(there):
+            block = proj[k * seqs : (k + 1) * seqs]
+            mine = jnp.where(ids == (j // shared).astype(F32), route, 0.0)
+            mine = jnp.sum(mine, axis=1, keepdims=True)
+            high = mine.astype(BF16).astype(F32)
+            tail = jnp.where(lane == 64, high, jnp.where(lane == 65, mine - high, block[:, 4 * half :]))
+            proj_send[j, :, : 4 * half] = block[:, : 4 * half].astype(BF16)
+            proj_send[j, :, 4 * half :] = tail.astype(BF16)
+            if offsets[k]:
+                swap_copy(proj_send, proj_recv, 0, j).start()
+
+    def near_projections(tree):
+        gather_relay(rows_a, 0, tree)
+        for k in (0, 1, 2, 3):
+            local[k].wait()
+            pair[k].wait()
+        first = dict.fromkeys(-s * o for s, o in first_arrivals(tree))
+        project(sorted(first, key=lambda o: -abs(o)) + [0])
+
+    def far_projections(tree):
+        first = first_arrivals(tree)
+        gather_last(rows_a, 0, tree)
+        project(sorted((-s * t for s, f, t in tree if (s, t) not in first), key=lambda o: -abs(o)))
+        gather_sent(rows_a, 0, tree)
+
+    by_core(0, near_projections)
+    local[8].wait()
+
+    def narrow(s, carry):
+        state16[s] = new_state_ref[s].astype(BF16)
+        return carry
+
+    lax.fori_loop(0, seqs, narrow, 0)
+    by_core(0, far_projections)
     proj_recv[chip] = proj_send[chip]
-    swap(proj_send, proj_recv, 0)()
+    swap_finish(proj_send, proj_recv, 0)
 
     maps = []
     for first in (0, 2 * thin):
@@ -374,7 +393,6 @@
     scaled = inputs * reps[:seqs]
     scaled_ref[...] = scaled
     maps_ref[...] = conv[:, width:]
-    local[8].wait()
 
     row = lax.broadcasted_iota(jnp.int32, (seqs, 1), 0)
     gated_in = []
@@ -384,9 +402,9 @@
         read_map = conv[:, first : first + state_width]
         read = jnp.zeros((seqs, group_width), F32)
         for s in range(seqs):
-            block = new_state_ref[s, g * per_group : (g + 1) * per_group].reshape(group_width, state_width)
+            block = state16[s, g * per_group : (g + 1) * per_group].reshape(group_width, state_width)
             picked = jnp.where(row == s, read_map, 0.0).astype(BF16)
-            read = read + nt_dot(picked, block.astype(BF16))
+            read = read + nt_dot(picked, block)
         cols = slice(g * group_width, (g + 1) * group_width)
         both = jnp.sum(write_map * read_map, axis=1, keepdims=True)
         read_out = reps[seqs : 2 * seqs, cols] * read + scaled[:, cols] * both + reps[2 * seqs :, cols] * inputs[:, cols]
@@ -396,7 +414,8 @@
     for j in range(chips):
         head_send[j] = gated[:, j * lanes : (j + 1) * lanes]
     head_recv[chip] = head_send[chip]
-    finish = swap(head_send, head_recv, 1)
+    for k in range(chips - 1, 0, -1):
+        swap_copy(head_send, head_recv, 1, at((k + 1) // 2 * (1 if k % 2 else -1))).start()
 
     def update(s, carry):
         rates = jnp.broadcast_to(rate_ref[pl.ds(s, 1)], (state_width, heads)).T
@@ -418,7 +437,7 @@
         return carry
 
     lax.fori_loop(0, seqs, update, 0)
-    finish()
+    swap_finish(head_send, head_recv, 1)
     local[4].wait()
     pair[4].wait()
 
@@ -426,12 +445,13 @@
     mixed = jnp.dot(heads_here, out_w[...], preferred_element_type=F32).reshape(chips, seqs, width)
     part32[...] = mixed
     part_send[0] = mixed.astype(BF16)
-    by_core(functools.partial(sum_at_owner, 0))
+    by_core(1, functools.partial(sum_at_owner, 0))
     residual = (hidden_buf[...].astype(F32) + total_ref[...]).astype(BF16)
     result_ref[...] = residual
     rows_e[chip] = rms_scale(residual.astype(F32), row_of(ffn_gain_buf)).astype(BF16)
-    by_core(functools.partial(gather_start, rows_e, 1))
-    by_core(functools.partial(gather_finish, rows_e, 1))
+    by_core(2, functools.partial(gather_start, rows_e, 1))
+    for part in (gather_relay, gather_last, gather_sent):
+        by_core(2, functools.partial(part, rows_e, 1))
     for k in (5, 6, 7):
         local[k].wait()
         pair[k].wait()
@@ -459,8 +479,19 @@
         return carry
 
     lax.fori_loop(0, width // tile, down_tile, 0, unroll=True)
-    by_core(functools.partial(sum_at_owner, 1))
+    by_core(3, functools.partial(sum_at_owner, 1))
     result_ref[...] = (result_ref[...].astype(F32) + total_ref[...]).astype(BF16)
+
+
+def store_kernel(result_in, state_in, conv_in, result_out, state_out, conv_out, sem):
+    count = state_in.shape[0]
+    copies = [pltpu.make_async_copy(state_in.at[k], state_out.at[k], sem.at[k]) for k in range(count)]
+    copies.append(pltpu.make_async_copy(result_in, result_out, sem.at[count]))
+    copies.append(pltpu.make_async_copy(conv_in, conv_out, sem.at[count + 1]))
+    for c in copies:
+        c.start()
+    for c in copies:
+        c.wait()
 
 
 def solution(mesh):
@@ -521,7 +552,7 @@
         vmem = pl.BlockSpec(memory_space=pltpu.VMEM)
         hbm = pl.BlockSpec(memory_space=pl.ANY)
         smalls = [operands[k] for k in (0, 1, 6, 7, 8, 9, 10, 11, 13, 15, 19, 20)]
-        edges = len(TREES[0])
+        edges = len(TREES[0][0])
         result, new_state, new_conv = pl.pallas_call(
             functools.partial(step_kernel, chips),
             out_shape=(
@@ -553,6 +584,7 @@
                 pltpu.VMEM((seqs, conv_dim - width), F32),
                 pltpu.VMEM((seqs, step_weight.shape[1]), F32),
                 pltpu.VMEM((seqs, width), F32),
+                pltpu.VMEM(mixer_state.shape, BF16),
                 *[pltpu.VMEM(value.shape, value.dtype) for value in smalls],
                 pltpu.SemaphoreType.DMA((len(smalls),)),
                 pltpu.SemaphoreType.DMA((9,)),
@@ -570,6 +602,16 @@
             ),
             name="step",
         )(*operands)
+        outs = (result, new_state, new_conv)
+        result, new_state, new_conv = pl.pallas_call(
+            store_kernel,
+            out_shape=tuple(jax.ShapeDtypeStruct(out.shape, out.dtype) for out in outs),
+            in_specs=[vmem] * 3,
+            out_specs=(hbm,) * 3,
+            scratch_shapes=[pltpu.SemaphoreType.DMA((seqs + 2,))],
+            compiler_params=pltpu.CompilerParams(vmem_limit_bytes=2**20),
+            name="store",
+        )(*outs)
         return result, new_state, new_conv.transpose(1, 0, 2)
 
     return jax.shard_map(

time: 96.6 us -> 94.2 us (0.975); the launches traced: 94.8 us -> 93.4 us
  local copies, waits for them, and re-layouts: 4.67 us -> 0 us
  Pallas kernels: 89.4 us -> 92.8 us
    unnamed x3 -> x0, local copies, waits for them, and re-layouts: 4.67 us -> none
    pallas_call x0 -> x1, Pallas kernels: none -> 3.4 us  [on_device(): pl.pallas_call(store_kernel, out_shape=tuple((jax.ShapeDtypeStruct(out.sh...]
where the time goes in v3:
time: 94.2 us; the launch traced here: 93.4 us
  Pallas kernels  92.8 us (99%)
    pallas_call x1, Pallas kernels, on_device(): pl.pallas_call(functools.partial(step_kernel, chips), out_shape=(pltpu.VM...  89.4 us
    pallas_call x1, Pallas kernels, on_device(): pl.pallas_call(store_kernel, out_shape=tuple((jax.ShapeDtypeStruct(out.sh...  3.4 us

profile of v3, /device:TPU:196, one launch (start us, length us, event | category | flops | bytes accessed | tf_op | source)
XLA Modules:
  0.0 93.4 jit_solution(7444121987453711152)
XLA Ops:
  0.6 89.4 %step.1 = (bf16[8,2048]{1,0:T(8,128)(2,1)S(1)}, f32[8,32,64,128]{3,2,1,0:T(8,128)S(1)}, bf16[3,8,3072]{2,1,0:T(8,128)(2,1)S(1)}) custom-call(bf16[8,2048]{1,0:T(8,128)(2,1)} %hidden_ref.1, bf16[2048]{0:T(1024)(128)(2,1)} %norm_gain_ref.1, bf16[64,2048]{1,0:T(8,128)(2,1)} %bitcast.12, bf16[64,2048]{1,0:T(8,128)(2,1)} %bitcast.13, bf16[16,2048]{1,0:T(8,128)(2,1)} %bitcast.16, ...), custom_call_target="tpu_custom_call" | custom-call | tf_op jit(solution)/shard_map/step/pallas_call | solution.py:556
  90.0 3.4 %store.1 = (bf16[8,2048]{1,0:T(8,128)(2,1)}, f32[8,32,64,128]{3,2,1,0:T(8,128)}, bf16[3,8,3072]{2,1,0:T(8,128)(2,1)}) custom-call(bf16[8,2048]{1,0:T(8,128)(2,1)S(1)} %get-tuple-element.9.result_in, f32[8,32,64,128]{3,2,1,0:T(8,128)S(1)} %get-tuple-element.10.state_in, bf16[3,8,3072]{2,1,0:T(8,128)(2,1)S(1)} %get-tuple-element.11.conv_in), custom_call_target="tpu_custom_call" | custom-call | tf_op jit(solution)/shard_map/store/pallas_call | solution.py:606

commit v4 on v3

--- a/solution.py
+++ b/solution.py
@@ -14,12 +14,12 @@
 BF16 = jnp.bfloat16
 norm_eps = 1e-06
 
-def both_ways(*edges):
-    return tuple((sign, f, t) for (f, t) in edges for sign in (1, -1) if not (t == 8 and sign < 0))
-
-
-A16 = both_ways((0, 5), (0, 2), (0, 1), (5, 8), (5, 7), (5, 6), (5, 4), (2, 3))
-T13 = both_ways((0, 3), (0, 1), (3, 6), (3, 4), (1, 2), (6, 8), (6, 7), (4, 5))
+def both_ways(far, *edges):
+    return tuple((sign, f, t) for (f, t) in edges for sign in (far, -far) if not (t == 8 and sign != far))
+
+
+A16 = both_ways(1, (0, 5), (0, 2), (0, 1), (5, 8), (5, 7), (5, 6), (5, 4), (2, 3))
+T13 = both_ways(-1, (0, 3), (0, 1), (3, 6), (3, 4), (1, 2), (6, 8), (6, 7), (4, 5))
 TREES = ((A16, T13), (A16, T13), (A16, T13), (A16, T13))
 GREET = sorted({way * abs(t - f) for pair in TREES for tree in pair for _, f, t in tree for way in (1, -1)})
 

time: 94.2 us -> 94.6 us (level)
  no operation moved by 1% of the time
where the time goes in v4:
time: 94.6 us; the launch traced here: 92.9 us
  Pallas kernels  92.3 us (98%)
    pallas_call x1, Pallas kernels, on_device(): pl.pallas_call(functools.partial(step_kernel, chips), out_shape=(pltpu.VM...  88.9 us
    pallas_call x1, Pallas kernels, on_device(): pl.pallas_call(store_kernel, out_shape=tuple((jax.ShapeDtypeStruct(out.sh...  3.4 us

profile of v4, /device:TPU:196, one launch (start us, length us, event | category | flops | bytes accessed | tf_op | source)
XLA Modules:
  0.0 92.9 jit_solution(1812536060119642126)
XLA Ops:
  0.6 88.9 %step.1 = (bf16[8,2048]{1,0:T(8,128)(2,1)S(1)}, f32[8,32,64,128]{3,2,1,0:T(8,128)S(1)}, bf16[3,8,3072]{2,1,0:T(8,128)(2,1)S(1)}) custom-call(bf16[8,2048]{1,0:T(8,128)(2,1)} %hidden_ref.1, bf16[2048]{0:T(1024)(128)(2,1)} %norm_gain_ref.1, bf16[64,2048]{1,0:T(8,128)(2,1)} %bitcast.12, bf16[64,2048]{1,0:T(8,128)(2,1)} %bitcast.13, bf16[16,2048]{1,0:T(8,128)(2,1)} %bitcast.16, ...), custom_call_target="tpu_custom_call" | custom-call | tf_op jit(solution)/shard_map/step/pallas_call | solution.py:556
  89.5 3.4 %store.1 = (bf16[8,2048]{1,0:T(8,128)(2,1)}, f32[8,32,64,128]{3,2,1,0:T(8,128)}, bf16[3,8,3072]{2,1,0:T(8,128)(2,1)}) custom-call(bf16[8,2048]{1,0:T(8,128)(2,1)S(1)} %get-tuple-element.9.result_in, f32[8,32,64,128]{3,2,1,0:T(8,128)S(1)} %get-tuple-element.10.state_in, bf16[3,8,3072]{2,1,0:T(8,128)(2,1)S(1)} %get-tuple-element.11.conv_in), custom_call_target="tpu_custom_call" | custom-call | tf_op jit(solution)/shard_map/store/pallas_call | solution.py:606
